TPU v7x, 32 devices: a whole 2x2x4 slice. The times are simulated.
32 devices in a mesh: ep: 8 (over z, x), tp: 4 (over y, core).
Axes of the slice: x: 2, y: 2, z: 4, core: 2. Of those that a mesh axis runs over, the one named last changes fastest.
Arguments:
- first_batch: bfloat16 [4096, 2048], P(('ep', 'tp')), may hold values from -6 to 6
- mixer_gain: float32 [2048], replicated, may hold values from 0.1 to 1.9
- mixer_in: bfloat16 [2048, 512], P(None, 'tp'), may hold values from -0.125 to 0.125
- group_maps: bfloat16 [8, 64, 64], replicated, may hold values from -0.75 to 0.75
- pool_scale: float32 [512], replicated, may hold values from 0.1 to 1.9
- mixer_out: bfloat16 [512, 2048], P('tp'), may hold values from -0.25 to 0.25
- second_batch: bfloat16 [1024, 2048], P('ep'), may hold values from -6 to 6
- expert_gain: float32 [2048], replicated, may hold values from 0.1 to 1.9
- expert_choice: int32 [1024, 2], P('ep'), may hold values from 0 to 7, all different within a row; in each aligned block of 128 rows (0 to 127, 128 to 255, ...) at most 64 rows name the same one
- route_scores: float32 [1024, 2], P('ep'), may hold values from -6 to 6
- expert_gate: bfloat16 [8, 2048, 3584], P('ep', None, 'tp'), may hold values from -0.125 to 0.125
- expert_up: bfloat16 [8, 2048, 3584], P('ep', None, 'tp'), may hold values from -0.125 to 0.125
- expert_down: bfloat16 [8, 3584, 2048], P('ep', 'tp'), may hold values from -0.09375 to 0.09375
Outputs:
- mixed_first: bfloat16 [4096, 2048], P(('ep', 'tp'))
- experts_second: bfloat16 [1024, 2048], P('ep')
Inputs may be any that keep to these rules, and one draw needn't show every extreme that they name: `expert_choice`: the two entries of a row differ. Within the rows of one device (aligned blocks of 128 rows) no expert is named more than 64 times, a bound that some block reaches there.
All inputs are finite; a program needn't handle non-finite values.
Results may differ from a plain program's by a relative error of at most 0.018.
Values may be sent and summed in bfloat16 or wider, within the bound.
A program may use at most 64 MiB of HBM per device.

v0:
```python
import jax
import jax.numpy as jnp
from jax import lax
from jax.sharding import PartitionSpec as P

GROUP = 64
SEQS = 1


epsilon = 1e-06


def extended(block, sides, width):
    for axis, dim in sides:
        count = lax.axis_size(axis)
        forward = [(i, i + 1) for i in range(count - 1)]
        backward = [(target, source) for source, target in forward]
        low = lax.ppermute(
            lax.slice_in_dim(block, block.shape[dim] - width, None, axis=dim), axis, forward
        )
        high = lax.ppermute(lax.slice_in_dim(block, 0, width, axis=dim), axis, backward)
        block = jnp.concatenate([low, block, high], axis=dim)
    return block


def rms_scale(values, gain):
    floats = values.astype(jnp.float32)
    factor = lax.rsqrt(jnp.mean(floats * floats, axis=-1, keepdims=True) + epsilon)
    return (floats * factor * gain).astype(jnp.bfloat16)


def mixer_half(first_batch, mixer_gain, mixer_in, group_maps, pool_scale, mixer_out):
    count_rows = first_batch.shape[0]
    normed = rms_scale(first_batch, mixer_gain)
    pooled_in = jnp.dot(
        normed,
        lax.all_gather(mixer_in, "tp", axis=1, tiled=True),
        preferred_element_type=jnp.float32,
    ).astype(jnp.bfloat16)
    channels = pooled_in.shape[1]
    padded = extended(pooled_in, ((("ep", "tp"), 0),), 8).astype(jnp.float32)
    devices = lax.axis_size("ep") * lax.axis_size("tp")
    seq_length = count_rows * devices // SEQS
    first_row = (lax.axis_index("ep") * lax.axis_size("tp") + lax.axis_index("tp")) * count_rows
    places = first_row + jnp.arange(count_rows, dtype=jnp.int32)
    own_seq = places // seq_length
    group_of = jnp.arange(channels, dtype=jnp.int32) // GROUP
    half_span = jnp.left_shift(jnp.ones_like(group_of), group_of % 4)
    window_sum = jnp.zeros((count_rows, channels), jnp.float32)
    window_count = jnp.zeros((count_rows, channels), jnp.float32)
    for offset in range(-8, 8):
        inside = (
            ((places + offset) // seq_length == own_seq)[:, None]
            & (offset >= -half_span)[None, :]
            & (offset < half_span)[None, :]
        )
        window_sum = window_sum + jnp.where(
            inside, padded[8 + offset : 8 + offset + count_rows], 0.0
        )
        window_count = window_count + inside.astype(jnp.float32)
    centred = (window_sum / window_count - padded[8 : 8 + count_rows]).astype(jnp.bfloat16)
    group_count = group_maps.shape[0]
    identity = jnp.eye(group_count, dtype=jnp.bfloat16)
    block_map = jnp.einsum("gcd,gh->gchd", group_maps, identity).reshape(channels, channels)
    grouped = (jnp.dot(centred, block_map, preferred_element_type=jnp.float32) * pool_scale).astype(
        jnp.bfloat16
    )
    mixed_out = jnp.dot(
        grouped,
        lax.all_gather(mixer_out, "tp", axis=0, tiled=True),
        preferred_element_type=jnp.float32,
    )
    return mixed_out.astype(jnp.bfloat16)


def expert_half(
    second_batch, expert_gain, expert_choice, route_scores, expert_gate, expert_up, expert_down
):
    row_count = second_batch.shape[0]
    model_width = second_batch.shape[1]
    experts = lax.axis_size("ep")
    tp_count = lax.axis_size("tp")
    capacity = 4 * row_count // experts
    share = capacity // tp_count
    normed = rms_scale(second_batch, expert_gain)
    chosen = expert_choice.reshape(-1)
    one_hot = (chosen[:, None] == jnp.arange(experts, dtype=jnp.int32)[None, :]).astype(jnp.int32)
    ranking = jnp.sum(jnp.cumsum(one_hot, axis=0) * one_hot, axis=1) - 1
    slot_place = ranking * experts + chosen
    source_row = jnp.arange(chosen.shape[0], dtype=jnp.int32) // expert_choice.shape[1]
    slot_table = jnp.zeros((capacity * experts,), jnp.int32).at[slot_place].set(source_row + 1)
    outgoing = jnp.where(
        (slot_table > 0)[:, None],
        normed[jnp.maximum(slot_table - 1, 0)],
        jnp.zeros((), jnp.bfloat16),
    )
    outgoing = outgoing.reshape(capacity, experts, model_width)
    portion = lax.dynamic_slice_in_dim(outgoing, lax.axis_index("tp") * share, share, 0)
    arrived_part = lax.all_to_all(portion, "ep", split_axis=1, concat_axis=1, tiled=True)
    arrived = lax.all_gather(arrived_part, "tp", axis=0, tiled=True)
    incoming = arrived.reshape(capacity * experts, model_width)
    gate_weight = expert_gate[0]
    up_weight = expert_up[0]
    down_weight = expert_down[0]
    gate_part = jnp.dot(incoming, gate_weight, preferred_element_type=jnp.float32)
    up_part = jnp.dot(incoming, up_weight, preferred_element_type=jnp.float32)
    hidden = (jax.nn.silu(gate_part) * up_part).astype(jnp.bfloat16)
    summed = lax.psum_scatter(
        jnp.dot(hidden, down_weight, preferred_element_type=jnp.float32).astype(jnp.bfloat16),
        "tp",
        scatter_dimension=0,
        tiled=True,
    )
    finished = summed.reshape(share, experts, model_width)
    returned = lax.all_to_all(finished, "ep", split_axis=1, concat_axis=1, tiled=True)
    every_slot = lax.all_gather(returned, "tp", axis=0, tiled=True).reshape(
        capacity * experts, model_width
    )
    picked = every_slot[slot_place].reshape(row_count, -1, model_width)
    weight_first = jax.nn.sigmoid(route_scores[:, 0] - route_scores[:, 1])[:, None]
    blended = weight_first * picked[:, 0].astype(jnp.float32) + (1.0 - weight_first) * picked[
        :, 1
    ].astype(jnp.float32)
    return blended.astype(jnp.bfloat16)


def per_device(
    first_batch,
    mixer_gain,
    mixer_in,
    group_maps,
    pool_scale,
    mixer_out,
    second_batch,
    expert_gain,
    expert_choice,
    route_scores,
    expert_gate,
    expert_up,
    expert_down,
):
    mixed_first = mixer_half(first_batch, mixer_gain, mixer_in, group_maps, pool_scale, mixer_out)
    experts_second = expert_half(
        second_batch, expert_gain, expert_choice, route_scores, expert_gate, expert_up, expert_down
    )
    return (mixed_first, experts_second)


def solution(mesh):
    placed = (
        P(("ep", "tp"), None),
        P(),
        P(None, "tp"),
        P(),
        P(),
        P("tp", None),
        P("ep", None),
        P(),
        P("ep", None),
        P("ep", None),
        P("ep", None, "tp"),
        P("ep", None, "tp"),
        P("ep", "tp", None),
    )
    return jax.shard_map(
        per_device,
        mesh=mesh,
        in_specs=placed,
        out_specs=(P(("ep", "tp"), None), P("ep", None)),
        check_vma=False,
    )
```

profile of v0, /device:TPU:11, one launch (start us, length us, event | category | flops | bytes accessed | tf_op | source)
XLA Modules:
  0.0 195.1 jit_solution(10836145895630367568)
XLA Ops:
  7.2 0.0 all-gather.9.cloned.1.call-start
  7.2 0.8 copy.22
  8.0 0.1 eq.156
  8.1 0.1 eq.152
  8.3 0.1 reshape.528
  8.4 0.6 reduce-window.6
  9.0 0.2 slice_reduce_fusion
  9.3 0.1 fusion.149
  9.4 1.4 scatter_custom_fusion
  10.9 1.2 fusion.19
  12.1 0.1 broadcast_in_dim.32
  12.2 0.1 copy.25
  12.3 1.2 fusion.21
  13.5 2.5 %gather_fusion = bf16[512,2048]{1,0:T(8,128)(2,1)S(1)} fusion(bf16[128,2048]{1,0:T(8,128)(2,1)S(1)} %fusion.21, s32[1024]{0:T(1024)S(1)} %pad_clamp_fusion.1), kind=kCustom, calls=%fused_computation | custom fusion | bytes 4196352 | tf_op jit(solution)/shard_map/gather | solution.py:94
  16.0 0.1 constant_dynamic-slice_fusion.1
  16.1 0.6 copy_select_fusion
  16.7 17.0 %all_to_all.10 = bf16[16,8,2048]{2,0,1:T(8,128)(2,1)S(1)} all-to-all(bf16[16,8,2048]{2,0,1:T(8,128)(2,1)S(1)} %copy_select_fusion), channel_id=1, replica_groups=mesh['ep'=8,'tp'=4] {'ep'}, dimensions={1} | all-to-all | bytes 1048576 | tf_op jit(solution)/shard_map/all_to_all | solution.py:99
  33.8 1.1 copy.27
  34.8 0.0 all-gather.9.cloned.1.call-update
  34.9 0.0 reduce-scatter.2.cloned.1.call-start
  34.9 25.1 %all-gather.9.cloned.1.call-done = bf16[64,8,2048]{2,1,0:T(8,128)(2,1)} async-done(((bf16[16,8,2048]{2,1,0:T(8,128)(2,1)}), bf16[64,8,2048]{2,1,0:T(8,128)(2,1)}) %all-gather.9.cloned.1.call-update) | async-done | bytes 2097168 | tf_op jit(solution)/shard_map/all_gather | solution.py:100
  60.0 6.4 %fusion.4 = f32[512,896]{1,0:T(8,128)} fusion(bf16[1,2048,896]{2,1,0:T(8,128)(2,1)} %param.23, bf16[64,8,2048]{2,1,0:T(8,128)(2,1)} %all-gather.9.cloned.1.call-done), kind=kOutput, calls=%fused_computation.7 | convolution fusion | flops 1879048192 | bytes 7602176 | tf_op jit(solution)/shard_map/dot_general | solution.py:105
  66.4 9.6 %fusion.6 = bf16[512,2048]{1,0:T(8,128)(2,1)} fusion(bf16[1,896,2048]{2,1,0:T(8,128)(2,1)} %param.25, f32[512,896]{1,0:T(8,128)} %fusion.4, bf16[1,2048,896]{2,1,0:T(8,128)(2,1)} %param.24, bf16[64,8,2048]{2,1,0:T(8,128)(2,1)S(1)} %copy-done.3), kind=kOutput, calls=%fused_computation.9 | convolution fusion | flops 3761897472 | bytes 13369344 | tf_op jit(solution)/shard_map/dot_general | solution.py:109
  76.0 0.0 reduce-scatter.2.cloned.1.call-update
  76.0 0.0 all-gather.5.cloned.1.call-start
  76.1 0.7 all-gather.5.cloned.1.call-update
  76.8 0.0 all-gather.7.cloned.1.call-start
  76.8 0.5 all-gather.7.cloned.1.call-update
  77.5 29.3 %reduce-scatter.2.cloned.1.call-done = bf16[128,2048]{1,0:T(8,128)(2,1)} async-done(((bf16[512,2048]{1,0:T(8,128)(2,1)}), bf16[128,2048]{1,0:T(8,128)(2,1)}) %reduce-scatter.2.cloned.1.call-update) | async-done | bytes 524304 | tf_op jit(solution)/shard_map/reduce_scatter | solution.py:108
  106.8 2.2 %copy.28 = bf16[16,8,2048]{2,0,1:T(8,128)(2,1)} copy(bf16[16,8,2048]{2,1,0:T(8,128)(2,1)} %bitcast.57) | data formatting | bytes 1048576 | tf_op jit(solution)/shard_map/reshape | solution.py:114
  109.0 5.6 %all-to-all-start.1 = ((bf16[16,8,2048]{2,0,1:T(8,128)(2,1)}), bf16[16,8,2048]{2,0,1:T(8,128)(2,1)S(1)}, u32[]{:S(2)}, u32[]{:S(2)}) async-start(bf16[16,8,2048]{2,0,1:T(8,128)(2,1)} %copy.28), calls=%async_computation.2 | async-start | bytes 1048576 | tf_op jit(solution)/shard_map/all_to_all | solution.py:115
  114.7 11.7 %all-to-all-done.1 = bf16[16,8,2048]{2,0,1:T(8,128)(2,1)S(1)} async-done(((bf16[16,8,2048]{2,0,1:T(8,128)(2,1)}), bf16[16,8,2048]{2,0,1:T(8,128)(2,1)S(1)}, u32[]{:S(2)}, u32[]{:S(2)}) %all-to-all-start.1) | async-done | bytes 524320 | tf_op jit(solution)/shard_map/all_to_all | solution.py:115
  126.5 1.1 copy.29
  127.7 0.2 fusion.16
  128.0 0.2 multiply_bitcast_fusion
  128.1 3.7 %all-gather.5.cloned.1.call-done = bf16[2048,512]{1,0:T(8,128)(2,1)} async-done(((bf16[2048,128]{1,0:T(8,128)(2,1)}), bf16[2048,512]{1,0:T(8,128)(2,1)}) %all-gather.5.cloned.1.call-update) | async-done | bytes 2097168 | tf_op jit(solution)/shard_map/all_gather | solution.py:37
  131.8 2.1 %convolution_convert_fusion.1 = bf16[128,512]{1,0:T(8,128)(2,1)S(1)} fusion(bf16[2048,512]{1,0:T(8,128)(2,1)} %all-gather.5.cloned.1.call-done, bf16[128,2048]{1,0:T(8,128)(2,1)S(1)} %copy-done, f32[2048]{0:T(1024)S(1)} %copy-done.4, f32[128]{0:T(128)S(1)} %add_rsqrt_fusion.1), kind=kOutput, calls=%fused_computation.20 | convolution fusion | flops 269549568 | bytes 2761216 | tf_op jit(solution)/shard_map/dot_general | solution.py:35
  133.9 2.3 %collective-permute-start = (bf16[8,512]{1,0:T(8,128)(2,1)S(1)}, bf16[8,512]{1,0:T(8,128)(2,1)S(1)}, u32[]{:S(2)}, u32[]{:S(2)}) collective-permute-start(bf16[8,512]{1,0:T(8,128)(2,1)S(1)} %get-tuple-element.6), channel_id=1, source_target_pairs={{0,1},{1,2},{2,3},{3,4},{4,5},{5,6},{6,7},{7,8},{8,9},{9,10},{10,1... | collective-permute-start | bytes 24584 | tf_op jit(solution)/shard_map/ppermute | solution.py:18
  136.2 2.2 %collective-permute-start.1 = (bf16[8,512]{1,0:T(8,128)(2,1)S(1)}, bf16[8,512]{1,0:T(8,128)(2,1)S(1)}, u32[]{:S(2)}, u32[]{:S(2)}) collective-permute-start(bf16[8,512]{1,0:T(8,128)(2,1)S(1)} %get-tuple-element.7), channel_id=1, source_target_pairs={{1,0},{2,1},{3,2},{4,3},{5,4},{6,5},{7,6},{8,7},{9,8},{10,9},{11,1... | collective-permute-start | bytes 24584 | tf_op jit(solution)/shard_map/ppermute | solution.py:21
  138.4 0.6 reshape.526
  139.1 2.1 %collective-permute-done.1 = bf16[8,512]{1,0:T(8,128)(2,1)S(1)} collective-permute-done((bf16[8,512]{1,0:T(8,128)(2,1)S(1)}, bf16[8,512]{1,0:T(8,128)(2,1)S(1)}, u32[]{:S(2)}, u32[]{:S(2)}) %collective-permute-start.1) | collective-permute-done | bytes 8224 | tf_op jit(solution)/shard_map/ppermute | solution.py:21
  141.2 14.5 %all-gather.7.cloned.1.call-done = bf16[512,2048]{1,0:T(8,128)(2,1)} async-done(((bf16[128,2048]{1,0:T(8,128)(2,1)}), bf16[512,2048]{1,0:T(8,128)(2,1)}) %all-gather.7.cloned.1.call-update) | async-done | bytes 2097168 | tf_op jit(solution)/shard_map/all_gather | solution.py:70
  155.8 4.2 %convolution_convert_fusion = bf16[128,2048]{1,0:T(8,128)(2,1)} fusion(bf16[512,2048]{1,0:T(8,128)(2,1)} %all-gather.7.cloned.1.call-done, bf16[512,512]{1,0:T(8,128)(2,1)S(1)} %reshape.526, f32[144,512]{1,0:T(8,128)S(1)} %maximum_convert_fusion, f32[512]{0:T(512)S(1)} %copy-done.5, f32[512]{0:T(512)S(1)} %get-tuple-element.53, ...), kind=kOutput, calls=%fused_computation.10 | convolution fusion | flops 342097920 | bytes 7367680 | tf_op jit(solution)/shard_map/dot_general | solution.py:68
  160.0 20.3 %all-gather.11.cloned.1.call-done = bf16[64,8,2048]{2,1,0:T(8,128)(2,1)} async-done(((bf16[16,8,2048]{2,1,0:T(8,128)(2,1)}), bf16[64,8,2048]{2,1,0:T(8,128)(2,1)}) %all-gather.11.cloned.1.call-update) | async-done | bytes 2097168 | tf_op jit(solution)/shard_map/all_gather | solution.py:116
  180.4 4.2 %gather_fusion.1 = bf16[256,2048]{1,0:T(8,128)(2,1)S(1)} fusion(bf16[512,2048]{1,0:T(8,128)(2,1)} %bitcast.55, s32[1024]{0:T(1024)S(1)} %pad_clamp_fusion), kind=kCustom, calls=%fused_computation.1 | custom fusion | bytes 2098176 | tf_op jit(solution)/shard_map/gather | solution.py:119
  184.6 0.7 reshape.532
  185.3 1.5 fusion.180
  186.8 1.8 fusion.23
  (56 shorter events, 0.5 us)
Async XLA Ops:
  7.2 52.9 %all-gather.9.cloned.1.call-start = ((), (), s32[]{:S(2)}) async-start(), calls=%async_computation.5 | async-start | bytes 2621440 | tf_op jit(solution)/shard_map/all_gather | solution.py:100
  34.9 71.9 %reduce-scatter.2.cloned.1.call-start = ((), (), s32[]{:S(2)}) async-start(), calls=%async_computation.6 | async-start | bytes 2621440 | tf_op jit(solution)/shard_map/reduce_scatter | solution.py:108
  60.0 6.4 %copy-start.3 = (bf16[64,8,2048]{2,1,0:T(8,128)(2,1)S(1)}, bf16[64,8,2048]{2,1,0:T(8,128)(2,1)}, u32[]{:S(2)}) copy-start(bf16[64,8,2048]{2,1,0:T(8,128)(2,1)} %all-gather.9.cloned.1.call-done) | copy-start | bytes 6291460
  76.0 55.8 %all-gather.5.cloned.1.call-start = ((), (), s32[]{:S(2)}) async-start(), calls=%async_computation.3 | async-start | bytes 2621440 | tf_op jit(solution)/shard_map/all_gather | solution.py:37
  76.8 51.0 %copy-start = (bf16[128,2048]{1,0:T(8,128)(2,1)S(1)}, bf16[128,2048]{1,0:T(8,128)(2,1)}, u32[]{:S(2)}) copy-start(bf16[128,2048]{1,0:T(8,128)(2,1)} %param.13) | copy-start | bytes 1572868
  76.8 79.0 %all-gather.7.cloned.1.call-start = ((), (), s32[]{:S(2)}) async-start(), calls=%async_computation.4 | async-start | bytes 2621440 | tf_op jit(solution)/shard_map/all_gather | solution.py:70
  106.8 21.1 %copy-start.2 = (f32[128,2]{0,1:T(2,128)S(1)}, f32[128,2]{0,1:T(2,128)}, u32[]{:S(2)}) copy-start(f32[128,2]{0,1:T(2,128)} %param.22) | copy-start | bytes 3076
  106.8 21.1 %copy-start.1 = (bf16[8,64,64]{2,1,0:T(8,128)(2,1)S(1)}, bf16[8,64,64]{2,1,0:T(8,128)(2,1)}, u32[]{:S(2)}) copy-start(bf16[8,64,64]{2,1,0:T(8,128)(2,1)} %param.16) | copy-start | bytes 196612
  109.0 22.8 %copy-start.4 = (f32[2048]{0:T(1024)S(1)}, f32[2048]{0:T(1024)}, u32[]{:S(2)}) copy-start(f32[2048]{0:T(1024)} %param.14) | copy-start | bytes 24580
  109.0 17.5 %all-to-all-start.1 = ((bf16[16,8,2048]{2,0,1:T(8,128)(2,1)}), bf16[16,8,2048]{2,0,1:T(8,128)(2,1)S(1)}, u32[]{:S(2)}, u32[]{:S(2)}) async-start(bf16[16,8,2048]{2,0,1:T(8,128)(2,1)} %copy.28), calls=%async_computation.2 | async-start | bytes 1048576 | tf_op jit(solution)/shard_map/all_to_all | solution.py:115
  114.6 65.8 %all-gather.11.cloned.1.call-start = ((), (), s32[]{:S(2)}) async-start(), calls=%async_computation.7 | async-start | bytes 2621440 | tf_op jit(solution)/shard_map/all_gather | solution.py:116
  128.1 27.7 %copy-start.5 = (f32[512]{0:T(512)S(1)}, f32[512]{0:T(512)}, u32[]{:S(2)}) copy-start(f32[512]{0:T(512)} %param.17) | copy-start | bytes 6148
  133.9 5.2 %collective-permute-start = (bf16[8,512]{1,0:T(8,128)(2,1)S(1)}, bf16[8,512]{1,0:T(8,128)(2,1)S(1)}, u32[]{:S(2)}, u32[]{:S(2)}) collective-permute-start(bf16[8,512]{1,0:T(8,128)(2,1)S(1)} %get-tuple-element.6), channel_id=1, source_target_pairs={{0,1},{1,2},{2,3},{3,4},{4,5},{5,6},{6,7},{7,8},{8,9},{9,10},{10,1... | collective-permute-start | bytes 24584 | tf_op jit(solution)/shard_map/ppermute | solution.py:18
  136.2 5.0 %collective-permute-start.1 = (bf16[8,512]{1,0:T(8,128)(2,1)S(1)}, bf16[8,512]{1,0:T(8,128)(2,1)S(1)}, u32[]{:S(2)}, u32[]{:S(2)}) collective-permute-start(bf16[8,512]{1,0:T(8,128)(2,1)S(1)} %get-tuple-element.7), channel_id=1, source_target_pairs={{1,0},{2,1},{3,2},{4,3},{5,4},{6,5},{7,6},{8,7},{9,8},{10,9},{11,1... | collective-permute-start | bytes 24584 | tf_op jit(solution)/shard_map/ppermute | solution.py:21
Sparse Core Ops, SparseCore 0:
  35.0 24.9 all-gather.8
  76.1 30.6 reduce-scatter.1
  108.4 23.3 all-gather.4
  133.2 22.5 all-gather.6
  157.8 22.5 all-gather.10
where the time goes:
time: 197 us; the launch traced here: 195 us
  waiting for transfers between devices  108 us (55%)
  matrix products  22.3 us (11%)
  local copies, waits for them, and re-layouts  17 us (9%)
  blocking collectives  17 us (9%)
  between operations  14.2 us (7%)
  starting transfers between devices  10.3 us (5%)
  other arithmetic  6.33 us (3%)
    reduce_scatter x1, waiting for transfers between devices, expert_half(): lax.psum_scatter(jnp.dot(hidden, down_weight, preferred_element_type=jnp....  29.3 us
    all_gather x1, waiting for transfers between devices, expert_half(): arrived = lax.all_gather(arrived_part, 'tp', axis=0, tiled=True)  25.1 us
    all_gather x1, waiting for transfers between devices, expert_half(): lax.all_gather(returned, 'tp', axis=0, tiled=True)  20.3 us
    all_to_all x1, blocking collectives, expert_half(): lax.all_to_all(portion, 'ep', split_axis=1, concat_axis=1, tiled=True)  17 us
    all_gather x1, waiting for transfers between devices, mixer_half(): lax.all_gather(mixer_out, 'tp', axis=0, tiled=True)  14.5 us
    all_to_all x1, waiting for transfers between devices, expert_half(): lax.all_to_all(finished, 'ep', split_axis=1, concat_axis=1, tiled=True)  11.7 us
    dot_general x1, matrix products, expert_half(): jnp.dot(hidden, down_weight, preferred_element_type=jnp.float32)  9.58 us
    dot_general x1, matrix products, expert_half(): jnp.dot(incoming, gate_weight, preferred_element_type=jnp.float32)  6.38 us
  transfers between devices with their start and end apart: 8, of which 7 were waited for; matrix products, arithmetic and copies ran while one was open for 6% of the time, Pallas kernels for 0%

commit v1 on v0

--- a/solution.py
+++ b/solution.py
@@ -1,6 +1,8 @@
 import jax
 import jax.numpy as jnp
 from jax import lax
+from jax.experimental import pallas as pl
+from jax.experimental.pallas import tpu as pltpu
 from jax.sharding import PartitionSpec as P
 
 GROUP = 64
@@ -124,6 +126,280 @@
     return blended.astype(jnp.bfloat16)
 
 
+MESH = pl.DeviceIdType.MESH
+VMEM_LIMIT = 40 * 1024 * 1024
+
+
+def greet(peers):
+    barrier = pltpu.get_barrier_semaphore()
+    for peer in peers:
+        pl.semaphore_signal(barrier, inc=1, device_id=peer, device_id_type=MESH)
+    pl.semaphore_wait(barrier, len(peers))
+
+
+def places_of(count):
+    row = lax.axis_index("ep")
+    col = lax.axis_index("tp")
+    partner = col + 1 - 2 * (col % 2)
+    across = (col + 2) % 4
+    others = [((row + k) % count, col) for k in range(1, count)]
+    return row, col, partner, across, others
+
+
+def remote(source, target, send, recv, device):
+    return pltpu.make_async_remote_copy(
+        src_ref=source,
+        dst_ref=target,
+        send_sem=send,
+        recv_sem=recv,
+        device_id=device,
+        device_id_type=MESH,
+    )
+
+
+def dispatch_kernel(count, portion, result, landed, send, recv, local):
+    row, col, partner, across, others = places_of(count)
+    greet(others + [(row, partner), (row, across)])
+    firsts = [None]
+    for k in range(1, count):
+        copy = remote(
+            portion.at[(row + k) % count], landed.at[row, col], send.at[0, k], recv.at[0, k],
+            ((row + k) % count, col),
+        )
+        copy.start()
+        firsts.append(copy)
+    own = pltpu.make_async_copy(portion.at[row], landed.at[row, col], local.at[0])
+    own.start()
+    own.wait()
+    sides, ys, corners = [], [], []
+    lag = 2
+    for k in range(count + lag):
+        if k < count:
+            source = (row + count - k) % count
+            if k > 0:
+                firsts[k].wait_recv()
+            block = landed.at[source, col]
+            y = remote(block, block, send.at[1, k], recv.at[1, k], (row, across))
+            y.start()
+            side = remote(block, block, send.at[2, k], recv.at[2, k], (row, partner))
+            side.start()
+            ys.append(y)
+            sides.append(side)
+        if k >= lag:
+            j = k - lag
+            source = (row + count - j) % count
+            ys[j].wait_recv()
+            block = landed.at[source, across]
+            corner = remote(block, block, send.at[3, j], recv.at[3, j], (row, partner))
+            corner.start()
+            corners.append(corner)
+    for k in range(count):
+        sides[k].wait_recv()
+        corners[k].wait_recv()
+    out = pltpu.make_async_copy(landed, result, local.at[1])
+    out.start()
+    for k in range(count):
+        if k > 0:
+            firsts[k].wait_send()
+        ys[k].wait_send()
+        sides[k].wait_send()
+        corners[k].wait_send()
+    out.wait()
+
+
+def dispatch(portion):
+    count, share, width = portion.shape
+    return pl.pallas_call(
+        lambda *refs: dispatch_kernel(count, *refs),
+        out_shape=jax.ShapeDtypeStruct((count, 4, share, width), portion.dtype),
+        in_specs=[pl.BlockSpec(memory_space=pltpu.VMEM)],
+        out_specs=pl.BlockSpec(memory_space=pl.ANY),
+        scratch_shapes=[
+            pltpu.VMEM((count, 4, share, width), portion.dtype),
+            pltpu.SemaphoreType.DMA((4, count)),
+            pltpu.SemaphoreType.DMA((4, count)),
+            pltpu.SemaphoreType.DMA((2,)),
+        ],
+        compiler_params=pltpu.CompilerParams(
+            collective_id=0, has_side_effects=True, vmem_limit_bytes=VMEM_LIMIT
+        ),
+        cost_estimate=pl.CostEstimate(flops=10**9, bytes_accessed=2**21, transcendentals=0),
+        name="dispatch",
+    )(portion)
+
+
+def combine_kernel(
+    count, part, weights, out, side_y, side_own, sums_y, from_y, sums, slots, pieces,
+    send, recv, send_out, recv_out,
+):
+    row, col, partner, across, others = places_of(count)
+    greet(others + [(row, partner), (row, across)])
+    quarter = part.shape[2] // 4
+    corner = (partner + 2) % 4
+
+    def columns(q):
+        return pl.ds(pl.multiple_of(q * quarter, quarter), quarter)
+
+    order = list(range(1, count)) + [0]
+    to_side, to_own, to_y, to_ep = {}, {}, {}, {}
+    for k in order:
+        target = (row + k) % count
+        to_side[k] = remote(
+            part.at[target, :, columns(corner)], side_y.at[k], send.at[0, k], recv.at[0, k],
+            (row, partner),
+        )
+        to_side[k].start()
+        to_own[k] = remote(
+            part.at[target, :, columns(partner)], side_own.at[k], send.at[1, k], recv.at[1, k],
+            (row, partner),
+        )
+        to_own[k].start()
+
+    def start_y(k):
+        to_y[k] = remote(
+            sums_y.at[k], from_y.at[k], send.at[2, k], recv.at[2, k], (row, across)
+        )
+        to_y[k].start()
+
+    def start_ep(k):
+        if k:
+            to_ep[k] = remote(
+                sums.at[k], slots.at[row], send.at[3, k], recv.at[3, k],
+                ((row + k) % count, col),
+            )
+            to_ep[k].start()
+
+    for i, k in enumerate(order):
+        target = (row + k) % count
+        to_side[k].wait_recv()
+        sums_y[k] = (
+            part[target, :, columns(across)].astype(jnp.float32)
+            + side_y[k].astype(jnp.float32)
+        ).astype(jnp.bfloat16)
+        if i:
+            start_y(order[i - 1])
+    to_own[order[0]].wait_recv()
+    start_y(order[-1])
+    for i, k in enumerate(order):
+        target = (row + k) % count
+        if i:
+            to_own[k].wait_recv()
+        mine = part[target, :, columns(col)].astype(jnp.float32) + side_own[k].astype(
+            jnp.float32
+        )
+        to_y[k].wait_recv()
+        total = (mine + from_y[k].astype(jnp.float32)).astype(jnp.bfloat16)
+        if k:
+            sums[k] = total
+            start_ep(k)
+        else:
+            slots[row] = total
+    table = weights[...]
+    high = table.astype(jnp.bfloat16)
+    low = (table - high.astype(jnp.float32)).astype(jnp.bfloat16)
+    for k in order[:-1]:
+        to_ep[k].wait_recv()
+    rows = slots[...].reshape(-1, quarter)
+    blended = jnp.dot(high, rows, preferred_element_type=jnp.float32) + jnp.dot(
+        low, rows, preferred_element_type=jnp.float32
+    )
+    pieces[col] = blended.astype(jnp.bfloat16)
+    own = pieces.at[col]
+    out_y = remote(own, own, send_out.at[0], recv_out.at[0], (row, across))
+    out_y.start()
+    out_side = remote(own, own, send_out.at[1], recv_out.at[1], (row, partner))
+    out_side.start()
+    out[:, columns(col)] = pieces[col]
+    out_y.wait_recv()
+    other = pieces.at[across]
+    out_corner = remote(other, other, send_out.at[2], recv_out.at[2], (row, partner))
+    out_corner.start()
+    out[:, columns(across)] = pieces[across]
+    out_side.wait_recv()
+    out[:, columns(partner)] = pieces[partner]
+    for k in order:
+        to_side[k].wait_send()
+        to_own[k].wait_send()
+        to_y[k].wait_send()
+        if k:
+            to_ep[k].wait_send()
+    out_corner.wait_recv()
+    out[:, columns(corner)] = pieces[corner]
+    out_y.wait_send()
+    out_side.wait_send()
+    out_corner.wait_send()
+
+
+def combine(part, weights):
+    count, capacity, width = part.shape
+    rows = weights.shape[0]
+    quarter = width // 4
+    chunk = pltpu.VMEM((count, capacity, quarter), jnp.bfloat16)
+    return pl.pallas_call(
+        lambda *refs: combine_kernel(count, *refs),
+        out_shape=jax.ShapeDtypeStruct((rows, width), jnp.bfloat16),
+        in_specs=[pl.BlockSpec(memory_space=pltpu.VMEM)] * 2,
+        out_specs=pl.BlockSpec(memory_space=pltpu.VMEM),
+        scratch_shapes=[chunk] * 6
+        + [
+            pltpu.VMEM((4, rows, quarter), jnp.bfloat16),
+            pltpu.SemaphoreType.DMA((4, count)),
+            pltpu.SemaphoreType.DMA((4, count)),
+            pltpu.SemaphoreType.DMA((3,)),
+            pltpu.SemaphoreType.DMA((3,)),
+        ],
+        compiler_params=pltpu.CompilerParams(
+            collective_id=1, has_side_effects=True, vmem_limit_bytes=VMEM_LIMIT
+        ),
+        cost_estimate=pl.CostEstimate(flops=10**9, bytes_accessed=2**21, transcendentals=0),
+        name="combine",
+    )(part, weights)
+
+
+def expert_half_kernels(
+    second_batch, expert_gain, expert_choice, route_scores, expert_gate, expert_up, expert_down
+):
+    row_count, model_width = second_batch.shape
+    experts = lax.axis_size("ep")
+    capacity = 4 * row_count // experts
+    share = capacity // 4
+    normed = rms_scale(second_batch, expert_gain)
+    names = jnp.arange(experts, dtype=jnp.int32)
+    is_first = expert_choice[:, 0:1] == names[None, :]
+    is_second = expert_choice[:, 1:2] == names[None, :]
+    named = is_first | is_second
+    rows = jnp.arange(row_count, dtype=jnp.int32)
+    before = (rows[None, :] < rows[:, None]).astype(jnp.bfloat16)
+    rank = jnp.dot(
+        before, named.astype(jnp.bfloat16), preferred_element_type=jnp.float32
+    ).astype(jnp.int32)
+    rank = jnp.where(named, rank, -1)
+    places = lax.axis_index("tp") * share + jnp.arange(share, dtype=jnp.int32)
+    pick = (rank.T[:, None, :] == places[None, :, None]).astype(jnp.bfloat16)
+    portion = (
+        jnp.dot(
+            pick.reshape(experts * share, row_count), normed, preferred_element_type=jnp.float32
+        )
+        .astype(jnp.bfloat16)
+        .reshape(experts, share, model_width)
+    )
+    incoming = dispatch(portion).reshape(experts * capacity, model_width)
+    gate_part = jnp.dot(incoming, expert_gate[0], preferred_element_type=jnp.float32)
+    up_part = jnp.dot(incoming, expert_up[0], preferred_element_type=jnp.float32)
+    hidden = (jax.nn.silu(gate_part) * up_part).astype(jnp.bfloat16)
+    part = jnp.dot(hidden, expert_down[0], preferred_element_type=jnp.float32).astype(
+        jnp.bfloat16
+    )
+    weight_first = jax.nn.sigmoid(route_scores[:, 0] - route_scores[:, 1])[:, None]
+    weight = jnp.where(is_first, weight_first, 1.0 - weight_first)
+    slot = jnp.arange(capacity, dtype=jnp.int32)
+    table = jnp.where(rank[:, :, None] == slot[None, None, :], weight[:, :, None], 0.0)
+    return combine(
+        part.reshape(experts, capacity, model_width),
+        table.reshape(row_count, experts * capacity),
+    )
+
+
 def per_device(
     first_batch,
     mixer_gain,
@@ -140,7 +416,8 @@
     expert_down,
 ):
     mixed_first = mixer_half(first_batch, mixer_gain, mixer_in, group_maps, pool_scale, mixer_out)
-    experts_second = expert_half(
+    small = lax.axis_size("tp") == 4 and lax.axis_size("ep") <= 8
+    experts_second = (expert_half_kernels if small else expert_half)(
         second_batch, expert_gain, expert_choice, route_scores, expert_gate, expert_up, expert_down
     )
     return (mixed_first, experts_second)

time: 197 us -> 113 us (0.57)
  waiting for transfers between devices: 108 us -> 1.4 us
  Pallas kernels: 0 us -> 61.6 us
  blocking collectives: 17 us -> 0 us
  local copies, waits for them, and re-layouts: 17 us -> 4.4 us
  starting transfers between devices: 10.3 us -> 4.4 us
  other arithmetic: 6.33 us -> 4.15 us
    pallas_call x0 -> x2, Pallas kernels: none -> 61.6 us  [the longest x1 30.9 us: combine(): pl.pallas_call(lambda *refs: combine_kernel(count, *refs), out_shape=jax....]
    all_gather x2 -> x0, waiting for transfers between devices: 45.4 us -> none  [the longest x1 25.1 us: expert_half(): arrived = lax.all_gather(arrived_part, 'tp', axis=0, tiled=True)]
    reduce_scatter x1 -> x0, waiting for transfers between devices: 29.3 us -> none  [expert_half(): lax.psum_scatter(jnp.dot(hidden, down_weight, preferred_element_type=jnp....]
    all_to_all x1 -> x0, blocking collectives: 17 us -> none  [expert_half(): lax.all_to_all(portion, 'ep', split_axis=1, concat_axis=1, tiled=True)]
    all_gather x1, waiting for transfers between devices: 14.5 us -> 0.02 us  [mixer_half(): lax.all_gather(mixer_out, 'tp', axis=0, tiled=True)]
    all_to_all x1 -> x0, waiting for transfers between devices: 11.7 us -> none  [expert_half(): lax.all_to_all(finished, 'ep', split_axis=1, concat_axis=1, tiled=True)]
    gather x2 -> x0, local copies, waits for them, and re-layouts: 6.69 us -> none  [the longest x1 4.22 us: expert_half(): picked = every_slot[slot_place].reshape(row_count, -1, model_width)]
    all_to_all x1 -> x0, starting transfers between devices: 5.61 us -> none  [expert_half(): lax.all_to_all(finished, 'ep', split_axis=1, concat_axis=1, tiled=True)]
  transfers between devices with their start and end apart: 8 -> 4, of which waited for: 7 -> 0; matrix products, arithmetic and copies ran while one was open for 6% -> 22% of each run, Pallas kernels for 0% -> 55%
where the time goes in v1:
time: 113 us
  Pallas kernels  61.6 us (55%)
  matrix products  22.3 us (20%)
  between operations  14.5 us (13%)
  local copies, waits for them, and re-layouts  4.4 us (4%)
  starting transfers between devices  4.4 us (4%)
  other arithmetic  4.15 us (4%)
  waiting for transfers between devices  1.4 us (1%)
    pallas_call x1, Pallas kernels, combine(): pl.pallas_call(lambda *refs: combine_kernel(count, *refs), out_shape=jax....  30.9 us
    pallas_call x1, Pallas kernels, dispatch(): pl.pallas_call(lambda *refs: dispatch_kernel(count, *refs), out_shape=jax...  30.7 us
    dot_general x1, matrix products, expert_half_kernels(): jnp.dot(hidden, expert_down[0], preferred_element_type=jnp.float32)  9.65 us
    dot_general x1, matrix products, expert_half_kernels(): jnp.dot(incoming, expert_gate[0], preferred_element_type=jnp.float32)  5.65 us
    dot_general x1, matrix products, mixer_half(): jnp.dot(grouped, lax.all_gather(mixer_out, 'tp', axis=0, tiled=True), pre...  4.26 us
    reduce_sum x2, other arithmetic, rms_scale(): jnp.mean(floats * floats, axis=-1, keepdims=True) + epsilon  2.46 us
    ppermute x1, starting transfers between devices, extended(): lax.ppermute(lax.slice_in_dim(block, block.shape[dim] - width, None, axis...  2.35 us
  transfers between devices with their start and end apart: 4, of which 0 were waited for; matrix products, arithmetic and copies ran while one was open for 22% of the time, Pallas kernels for 55%

profile of v1, /device:TPU:11, one launch (start us, length us, event | category | flops | bytes accessed | tf_op | source)
XLA Modules:
  0.0 112.7 jit_solution(12098988184310742728)
XLA Ops:
  7.2 0.0 copy-start.1
  7.2 0.0 copy-start.5
  7.2 0.0 copy-start.4
  7.2 0.0 all-gather.3.cloned.1.call-start
  7.2 0.7 all-gather.3.cloned.1.call-update
  7.9 0.0 all-gather.5.cloned.1.call-start
  8.0 0.7 all-gather.5.cloned.1.call-update
  9.1 1.2 %fusion.12 = f32[128]{0:T(128)S(1)} fusion(bf16[128,2048]{1,0:T(8,128)(2,1)} %param.13), kind=kLoop, calls=%fused_computation.18 | loop fusion | flops 786304 | bytes 524800 | tf_op jit(solution)/shard_map/reduce_sum | solution.py:30
  10.3 0.8 slice_bitcast_fusion.1
  11.1 0.1 eq.232
  11.2 1.2 %fusion.15 = f32[128]{0:T(128)S(1)} fusion(bf16[128,2048]{1,0:T(8,128)(2,1)} %param.19), kind=kLoop, calls=%fused_computation.21 | loop fusion | flops 786304 | bytes 524800 | tf_op jit(solution)/shard_map/reduce_sum | solution.py:30
  12.4 0.1 bitcast_select_fusion
  12.6 0.0 copy-done.5
  12.6 0.1 bitcast_compare_fusion
  12.7 0.0 copy-done.1
  12.7 0.0 copy-done.4
  12.8 0.4 convolution_convert_fusion
  13.1 30.7 %dispatch.1 = bf16[8,4,16,2048]{3,2,1,0:T(8,128)(2,1)S(1)} custom-call(bf16[8,16,2048]{2,1,0:T(8,128)(2,1)S(1)} %bitcast.41), custom_call_target="tpu_custom_call" | custom-call | flops 1000000000 | bytes 2097152 | tf_op jit(solution)/shard_map/dispatch/pallas_call | solution.py:212
  43.8 0.0 copy-start.3
  43.9 0.1 copy.17
  44.0 0.1 copy.18
  44.2 0.1 eq.238
  44.3 0.4 copy-done.3
  44.7 1.2 %multiply_bitcast_fusion = bf16[8,64,8,64]{3,2,1,0:T(8,128)(2,1)} fusion(bf16[8,64,64]{2,1,0:T(8,128)(2,1)S(1)} %copy-done.3, bf16[8,8]{1,0:T(8,128)(2,1)S(1)} %fusion.145), kind=kLoop, calls=%fused_computation.24 | loop fusion | flops 262144 | bytes 589952 | tf_op jit(solution)/shard_map/gcd,gh->gchd/transpose | solution.py:66
  46.0 5.7 %fusion.4 = f32[512,896]{1,0:T(8,128)} fusion(bf16[512,2048]{1,0:T(8,128)(2,1)S(1)} %bitcast.42, bf16[1,2048,896]{2,1,0:T(8,128)(2,1)} %param.23), kind=kOutput, calls=%fused_computation.4 | convolution fusion | flops 1879048192 | bytes 7602176 | tf_op jit(solution)/shard_map/dot_general | solution.py:387
  51.6 0.0 copy-start.2
  51.6 0.0 copy-start.6
  51.6 9.7 %fusion.6 = bf16[512,2048]{1,0:T(8,128)(2,1)} fusion(bf16[1,896,2048]{2,1,0:T(8,128)(2,1)} %param.25, f32[512,896]{1,0:T(8,128)} %fusion.4, bf16[512,2048]{1,0:T(8,128)(2,1)S(1)} %bitcast.43, bf16[1,2048,896]{2,1,0:T(8,128)(2,1)} %param.24), kind=kOutput, calls=%fused_computation.6 | convolution fusion | flops 3761897472 | bytes 13369344 | tf_op jit(solution)/shard_map/dot_general | solution.py:390
  61.3 0.0 copy-start
  61.3 0.0 all-gather.3.cloned.1.call-done
  61.3 0.0 copy-done.2
  61.3 0.0 copy-done.6
  61.3 2.2 %convolution_convert_fusion.2 = bf16[128,512]{1,0:T(8,128)(2,1)S(1)} fusion(bf16[2048,512]{1,0:T(8,128)(2,1)} %all-gather.3.cloned.1.call-done, bf16[128,2048]{1,0:T(8,128)(2,1)S(1)} %copy-done.2, f32[2048]{0:T(1024)S(1)} %copy-done.6, f32[128]{0:T(128)S(1)} %add_rsqrt_fusion.1), kind=kOutput, calls=%fused_computation.16 | convolution fusion | flops 269549568 | bytes 2761216 | tf_op jit(solution)/shard_map/dot_general | solution.py:37
  63.5 2.4 %collective-permute-start = (bf16[8,512]{1,0:T(8,128)(2,1)S(1)}, bf16[8,512]{1,0:T(8,128)(2,1)S(1)}, u32[]{:S(2)}, u32[]{:S(2)}) collective-permute-start(bf16[8,512]{1,0:T(8,128)(2,1)S(1)} %get-tuple-element.4), channel_id=1, source_target_pairs={{0,1},{1,2},{2,3},{3,4},{4,5},{5,6},{6,7},{7,8},{8,9},{9,10},{10,1... | collective-permute-start | bytes 24584 | tf_op jit(solution)/shard_map/ppermute | solution.py:20
  65.9 2.0 %collective-permute-start.1 = (bf16[8,512]{1,0:T(8,128)(2,1)S(1)}, bf16[8,512]{1,0:T(8,128)(2,1)S(1)}, u32[]{:S(2)}, u32[]{:S(2)}) collective-permute-start(bf16[8,512]{1,0:T(8,128)(2,1)S(1)} %get-tuple-element.5), channel_id=1, source_target_pairs={{1,0},{2,1},{3,2},{4,3},{5,4},{6,5},{7,6},{8,7},{9,8},{10,9},{11,1... | collective-permute-start | bytes 24584 | tf_op jit(solution)/shard_map/ppermute | solution.py:23
  67.9 0.0 copy-done
  67.9 0.0 copy-start.7
  67.9 30.9 %combine.1 = bf16[128,2048]{1,0:T(8,128)(2,1)S(1)} custom-call(bf16[8,64,2048]{2,1,0:T(8,128)(2,1)S(1)} %bitcast.44, f32[128,512]{1,0:T(8,128)S(1)} %compare_select_fusion.refs_1_), custom_call_target="tpu_custom_call" | custom-call | flops 1000000000 | bytes 2097152 | tf_op jit(solution)/shard_map/combine/pallas_call | solution.py:338
  98.8 1.9 %reshape.526 = bf16[512,512]{1,0:T(8,128)(2,1)S(1)} reshape(bf16[8,64,8,64]{3,2,1,0:T(8,128)(2,1)} %multiply_bitcast_fusion) | data formatting | bytes 1048576 | tf_op jit(solution)/shard_map/reshape | solution.py:66
  100.7 0.0 collective-permute-done
  100.7 0.0 collective-permute-done.1
  100.8 0.0 all-gather.5.cloned.1.call-done
  100.8 0.0 copy-done.7
  100.8 4.3 %convolution_convert_fusion.1 = bf16[128,2048]{1,0:T(8,128)(2,1)} fusion(bf16[512,2048]{1,0:T(8,128)(2,1)} %all-gather.5.cloned.1.call-done, bf16[512,512]{1,0:T(8,128)(2,1)S(1)} %reshape.526, f32[144,512]{1,0:T(8,128)S(1)} %maximum_convert_fusion, f32[512]{0:T(512)S(1)} %copy-done.7, f32[512]{0:T(512)S(1)} %get-tuple-element.55, ...), kind=kOutput, calls=%fused_computation.8 | convolution fusion | flops 342097920 | bytes 7367680 | tf_op jit(solution)/shard_map/dot_general | solution.py:70
  105.1 0.8 copy.22
  (38 shorter events, 0.4 us)
Async XLA Ops:
  7.2 5.6 %copy-start.1 = (bf16[128,2048]{1,0:T(8,128)(2,1)S(1)}, bf16[128,2048]{1,0:T(8,128)(2,1)}, u32[]{:S(2)}) copy-start(bf16[128,2048]{1,0:T(8,128)(2,1)} %param.19) | copy-start | bytes 1572868
  7.2 5.4 %copy-start.5 = (f32[128,2]{0,1:T(2,128)S(1)}, f32[128,2]{0,1:T(2,128)}, u32[]{:S(2)}) copy-start(f32[128,2]{0,1:T(2,128)} %param.22) | copy-start | bytes 3076
  7.2 5.6 %copy-start.4 = (f32[2048]{0:T(1024)S(1)}, f32[2048]{0:T(1024)}, u32[]{:S(2)}) copy-start(f32[2048]{0:T(1024)} %param.20) | copy-start | bytes 24580
  7.2 54.1 %all-gather.3.cloned.1.call-start = ((), (), s32[]{:S(2)}) async-start(), calls=%async_computation | async-start | bytes 2621440 | tf_op jit(solution)/shard_map/all_gather | solution.py:39
  7.9 92.9 %all-gather.5.cloned.1.call-start = ((), (), s32[]{:S(2)}) async-start(), calls=%async_computation.1 | async-start | bytes 2621440 | tf_op jit(solution)/shard_map/all_gather | solution.py:72
  43.8 0.9 copy-start.3
  51.6 9.7 %copy-start.2 = (bf16[128,2048]{1,0:T(8,128)(2,1)S(1)}, bf16[128,2048]{1,0:T(8,128)(2,1)}, u32[]{:S(2)}) copy-start(bf16[128,2048]{1,0:T(8,128)(2,1)} %param.13) | copy-start | bytes 1572868
  51.6 9.7 %copy-start.6 = (f32[2048]{0:T(1024)S(1)}, f32[2048]{0:T(1024)}, u32[]{:S(2)}) copy-start(f32[2048]{0:T(1024)} %param.14) | copy-start | bytes 24580
  61.3 6.6 %copy-start = (bf16[512,2048]{1,0:T(8,128)(2,1)S(1)}, bf16[512,2048]{1,0:T(8,128)(2,1)}, u32[]{:S(2)}) copy-start(bf16[512,2048]{1,0:T(8,128)(2,1)} %fusion.6) | copy-start | bytes 6291460
  63.5 37.2 %collective-permute-start = (bf16[8,512]{1,0:T(8,128)(2,1)S(1)}, bf16[8,512]{1,0:T(8,128)(2,1)S(1)}, u32[]{:S(2)}, u32[]{:S(2)}) collective-permute-start(bf16[8,512]{1,0:T(8,128)(2,1)S(1)} %get-tuple-element.4), channel_id=1, source_target_pairs={{0,1},{1,2},{2,3},{3,4},{4,5},{5,6},{6,7},{7,8},{8,9},{9,10},{10,1... | collective-permute-start | bytes 24584 | tf_op jit(solution)/shard_map/ppermute | solution.py:20
  65.9 34.8 %collective-permute-start.1 = (bf16[8,512]{1,0:T(8,128)(2,1)S(1)}, bf16[8,512]{1,0:T(8,128)(2,1)S(1)}, u32[]{:S(2)}, u32[]{:S(2)}) collective-permute-start(bf16[8,512]{1,0:T(8,128)(2,1)S(1)} %get-tuple-element.5), channel_id=1, source_target_pairs={{1,0},{2,1},{3,2},{4,3},{5,4},{6,5},{7,6},{8,7},{9,8},{10,9},{11,1... | collective-permute-start | bytes 24584 | tf_op jit(solution)/shard_map/ppermute | solution.py:23
  67.9 32.9 %copy-start.7 = (f32[512]{0:T(512)S(1)}, f32[512]{0:T(512)}, u32[]{:S(2)}) copy-start(f32[512]{0:T(512)} %param.17) | copy-start | bytes 6148
Sparse Core Ops, SparseCore 0:
  9.6 34.0 all-gather.2
  45.3 20.7 all-gather.4

commit v2 on v1

--- a/solution.py
+++ b/solution.py
@@ -36,7 +36,7 @@
     normed = rms_scale(first_batch, mixer_gain)
     pooled_in = jnp.dot(
         normed,
-        lax.all_gather(mixer_in, "tp", axis=1, tiled=True),
+        mixer_in,
         preferred_element_type=jnp.float32,
     ).astype(jnp.bfloat16)
     channels = pooled_in.shape[1]
@@ -69,7 +69,7 @@
     )
     mixed_out = jnp.dot(
         grouped,
-        lax.all_gather(mixer_out, "tp", axis=0, tiled=True),
+        mixer_out,
         preferred_element_type=jnp.float32,
     )
     return mixed_out.astype(jnp.bfloat16)
@@ -157,7 +157,10 @@
     )
 
 
-def dispatch_kernel(count, portion, result, landed, send, recv, local):
+def dispatch_kernel(
+    count, portion, w_in, w_out, result, full_in, full_out, landed, held_in, held_out,
+    send, recv, local, send_w, recv_w,
+):
     row, col, partner, across, others = places_of(count)
     greet(others + [(row, partner), (row, across)])
     firsts = [None]
@@ -168,6 +171,27 @@
         )
         copy.start()
         firsts.append(copy)
+
+    def piece(which, index):
+        if which == 0:
+            size = w_in.shape[1]
+            return held_in.at[:, pl.ds(pl.multiple_of(index * size, size), size)]
+        size = w_out.shape[0]
+        return held_out.at[pl.ds(pl.multiple_of(index * size, size), size), :]
+
+    weights = []
+    for which, source in ((0, w_in), (1, w_out)):
+        here = pltpu.make_async_copy(source, piece(which, col), local.at[2 + which])
+        here.start()
+        y = remote(
+            source, piece(which, col), send_w.at[which, 0], recv_w.at[which, 0], (row, across)
+        )
+        y.start()
+        side = remote(
+            source, piece(which, col), send_w.at[which, 1], recv_w.at[which, 1], (row, partner)
+        )
+        side.start()
+        weights.append((here, y, side))
     own = pltpu.make_async_copy(portion.at[row], landed.at[row, col], local.at[0])
     own.start()
     own.wait()
@@ -198,6 +222,27 @@
         corners[k].wait_recv()
     out = pltpu.make_async_copy(landed, result, local.at[1])
     out.start()
+    corner_w = []
+    for which in (0, 1):
+        weights[which][1].wait_recv()
+        block = piece(which, across)
+        copy = remote(block, block, send_w.at[which, 2], recv_w.at[which, 2], (row, partner))
+        copy.start()
+        corner_w.append(copy)
+    outs = []
+    for which, held, full in ((0, held_in, full_in), (1, held_out, full_out)):
+        here, y, side = weights[which]
+        here.wait()
+        side.wait_recv()
+        corner_w[which].wait_recv()
+        copy = pltpu.make_async_copy(held, full, local.at[4 + which])
+        copy.start()
+        outs.append(copy)
+    for which in (0, 1):
+        weights[which][1].wait_send()
+        weights[which][2].wait_send()
+        corner_w[which].wait_send()
+        outs[which].wait()
     for k in range(count):
         if k > 0:
             firsts[k].wait_send()
@@ -207,25 +252,35 @@
     out.wait()
 
 
-def dispatch(portion):
+def dispatch(portion, w_in, w_out):
     count, share, width = portion.shape
+    shape_in = (w_in.shape[0], 4 * w_in.shape[1])
+    shape_out = (4 * w_out.shape[0], w_out.shape[1])
     return pl.pallas_call(
         lambda *refs: dispatch_kernel(count, *refs),
-        out_shape=jax.ShapeDtypeStruct((count, 4, share, width), portion.dtype),
-        in_specs=[pl.BlockSpec(memory_space=pltpu.VMEM)],
-        out_specs=pl.BlockSpec(memory_space=pl.ANY),
+        out_shape=(
+            jax.ShapeDtypeStruct((count, 4, share, width), portion.dtype),
+            jax.ShapeDtypeStruct(shape_in, w_in.dtype),
+            jax.ShapeDtypeStruct(shape_out, w_out.dtype),
+        ),
+        in_specs=[pl.BlockSpec(memory_space=pltpu.VMEM)] * 3,
+        out_specs=[pl.BlockSpec(memory_space=pl.ANY)] * 3,
         scratch_shapes=[
             pltpu.VMEM((count, 4, share, width), portion.dtype),
+            pltpu.VMEM(shape_in, w_in.dtype),
+            pltpu.VMEM(shape_out, w_out.dtype),
             pltpu.SemaphoreType.DMA((4, count)),
             pltpu.SemaphoreType.DMA((4, count)),
-            pltpu.SemaphoreType.DMA((2,)),
+            pltpu.SemaphoreType.DMA((6,)),
+            pltpu.SemaphoreType.DMA((2, 3)),
+            pltpu.SemaphoreType.DMA((2, 3)),
         ],
         compiler_params=pltpu.CompilerParams(
             collective_id=0, has_side_effects=True, vmem_limit_bytes=VMEM_LIMIT
         ),
         cost_estimate=pl.CostEstimate(flops=10**9, bytes_accessed=2**21, transcendentals=0),
         name="dispatch",
-    )(portion)
+    )(portion, w_in, w_out)
 
 
 def combine_kernel(
@@ -357,7 +412,8 @@
 
 
 def expert_half_kernels(
-    second_batch, expert_gain, expert_choice, route_scores, expert_gate, expert_up, expert_down
+    second_batch, expert_gain, expert_choice, route_scores, expert_gate, expert_up, expert_down,
+    mixer_in, mixer_out,
 ):
     row_count, model_width = second_batch.shape
     experts = lax.axis_size("ep")
@@ -383,7 +439,8 @@
         .astype(jnp.bfloat16)
         .reshape(experts, share, model_width)
     )
-    incoming = dispatch(portion).reshape(experts * capacity, model_width)
+    arrived, full_in, full_out = dispatch(portion, mixer_in, mixer_out)
+    incoming = arrived.reshape(experts * capacity, model_width)
     gate_part = jnp.dot(incoming, expert_gate[0], preferred_element_type=jnp.float32)
     up_part = jnp.dot(incoming, expert_up[0], preferred_element_type=jnp.float32)
     hidden = (jax.nn.silu(gate_part) * up_part).astype(jnp.bfloat16)
@@ -394,10 +451,11 @@
     weight = jnp.where(is_first, weight_first, 1.0 - weight_first)
     slot = jnp.arange(capacity, dtype=jnp.int32)
     table = jnp.where(rank[:, :, None] == slot[None, None, :], weight[:, :, None], 0.0)
-    return combine(
+    blended = combine(
         part.reshape(experts, capacity, model_width),
         table.reshape(row_count, experts * capacity),
     )
+    return blended, full_in, full_out
 
 
 def per_device(
@@ -415,10 +473,17 @@
     expert_up,
     expert_down,
 ):
-    mixed_first = mixer_half(first_batch, mixer_gain, mixer_in, group_maps, pool_scale, mixer_out)
-    small = lax.axis_size("tp") == 4 and lax.axis_size("ep") <= 8
-    experts_second = (expert_half_kernels if small else expert_half)(
+    routed = (
         second_batch, expert_gain, expert_choice, route_scores, expert_gate, expert_up, expert_down
+    )
+    if lax.axis_size("tp") == 4 and lax.axis_size("ep") <= 8:
+        experts_second, full_in, full_out = expert_half_kernels(*routed, mixer_in, mixer_out)
+    else:
+        experts_second = expert_half(*routed)
+        full_in = lax.all_gather(mixer_in, "tp", axis=1, tiled=True)
+        full_out = lax.all_gather(mixer_out, "tp", axis=0, tiled=True)
+    mixed_first = mixer_half(
+        first_batch, mixer_gain, full_in, group_maps, pool_scale, full_out
     )
     return (mixed_first, experts_second)
 

time: 113 us -> 120 us (1.062)
  between operations: 14.5 us -> 0.99 us
  Pallas kernels: 61.6 us -> 73.8 us
  other arithmetic: 4.15 us -> 11.9 us
  local copies, waits for them, and re-layouts: 4.4 us -> 7.01 us
  matrix products: 22.3 us -> 20.7 us
  waiting for transfers between devices: 1.4 us -> 0.01 us
    pallas_call x1, Pallas kernels: 30.7 us -> 43 us  [dispatch(): pl.pallas_call(lambda *refs: dispatch_kernel(count, *refs), out_shape=(ja...]
    le x14, other arithmetic: 0.12 us -> 7.01 us  [mixer_half(): offset >= -half_span]
    unnamed x17 -> x23, local copies, waits for them, and re-layouts: 1.28 us -> 3.87 us
    dot_general x2, matrix products: 6.51 us -> 3.93 us  [the longest x1 3.44 us: mixer_half(): mixed_out = jnp.dot(grouped, mixer_out, preferred_element_type=jnp.float32)]
    unnamed x2 -> x0, waiting for transfers between devices: 1.38 us -> none
  transfers between devices with their start and end apart: 4 -> 2, of which waited for: 0 -> 0; matrix products, arithmetic and copies ran while one was open for 22% -> 22% of each run, Pallas kernels for 55% -> 26%
where the time goes in v2:
time: 120 us; the launch traced here: 119 us
  Pallas kernels  73.8 us (62%)
  matrix products  20.7 us (17%)
  other arithmetic  11.9 us (10%)
  local copies, waits for them, and re-layouts  7.01 us (6%)
  starting transfers between devices  5.13 us (4%)
    pallas_call x1, Pallas kernels, dispatch(): pl.pallas_call(lambda *refs: dispatch_kernel(count, *refs), out_shape=(ja...  43 us
    pallas_call x1, Pallas kernels, combine(): pl.pallas_call(lambda *refs: combine_kernel(count, *refs), out_shape=jax....  30.7 us
    dot_general x1, matrix products, expert_half_kernels(): jnp.dot(hidden, expert_down[0], preferred_element_type=jnp.float32)  9.54 us
    le x14, other arithmetic, mixer_half(): offset >= -half_span  7.01 us
    dot_general x1, matrix products, expert_half_kernels(): jnp.dot(incoming, expert_gate[0], preferred_element_type=jnp.float32)  5.65 us
    unnamed x23, local copies, waits for them, and re-layouts  3.87 us
    dot_general x1, matrix products, mixer_half(): mixed_out = jnp.dot(grouped, mixer_out, preferred_element_type=jnp.float32)  3.44 us
    ppermute x1, starting transfers between devices, extended(): lax.ppermute(lax.slice_in_dim(block, block.shape[dim] - width, None, axis...  3.21 us
  transfers between devices with their start and end apart: 2, of which 0 were waited for; matrix products, arithmetic and copies ran while one was open for 22% of the time, Pallas kernels for 26%

profile of v2, /device:TPU:11, one launch (start us, length us, event | category | flops | bytes accessed | tf_op | source)
XLA Modules:
  0.0 119.5 jit_solution(744975433792438365)
XLA Ops:
  0.6 0.0 copy-start
  0.6 0.0 copy-start.1
  0.7 0.8 slice_bitcast_fusion.1
  1.4 0.1 eq.217
  1.5 1.2 %fusion.15 = f32[128]{0:T(128)S(1)} fusion(bf16[128,2048]{1,0:T(8,128)(2,1)} %param.19), kind=kLoop, calls=%fused_computation.21 | loop fusion | flops 786304 | bytes 524800 | tf_op jit(solution)/shard_map/reduce_sum | solution.py:30
  2.8 1.2 %fusion.12 = f32[128]{0:T(128)S(1)} fusion(bf16[128,2048]{1,0:T(8,128)(2,1)} %param.13), kind=kLoop, calls=%fused_computation.18 | loop fusion | flops 786304 | bytes 524800 | tf_op jit(solution)/shard_map/reduce_sum | solution.py:30
  4.0 0.1 bitcast_select_fusion
  4.2 0.1 bitcast_compare_fusion
  4.3 1.4 %convolution_convert_fusion.1 = bf16[128,2048]{1,0:T(8,128)(2,1)S(1)} fusion(pred[128,128]{1,0:T(32,128)(4,1)S(1)} %bitcast_compare_fusion, bf16[128,2048]{1,0:T(8,128)(2,1)} %param.19, f32[2048]{0:T(1024)} %param.20, f32[128]{0:T(128)S(1)} %add_rsqrt_fusion), kind=kOutput, calls=%fused_computation.8 | convolution fusion | flops 68419584 | bytes 1073664 | tf_op jit(solution)/shard_map/dot_general | solution.py:436
  5.7 0.0 copy-start.5
  5.7 0.0 copy-start.9
  5.7 0.0 copy-done
  5.7 0.0 copy-done.1
  5.7 43.0 %dispatch.1 = (bf16[8,4,16,2048]{3,2,1,0:T(8,128)(2,1)S(1)}, bf16[2048,512]{1,0:T(8,128)(2,1)S(1)}, bf16[512,2048]{1,0:T(8,128)(2,1)S(1)}) custom-call(bf16[8,16,2048]{2,1,0:T(8,128)(2,1)S(1)} %bitcast.41, bf16[2048,128]{1,0:T(8,128)(2,1)S(1)} %copy-done, bf16[128,2048]{1,0:T(8,128)(2,1)S(1)} %copy-done.1), custom_call_target="tpu_custom_call" | custom-call | flops 1000000000 | bytes 2097152 | tf_op jit(solution)/shard_map/dispatch/pallas_call | solution.py:259
  48.8 0.0 copy-start.8
  48.8 0.0 copy-start.7
  48.8 0.5 convolution_convert_fusion.2
  49.3 0.8 copy-done.3
  50.1 0.7 copy-done.6
  50.8 3.2 %collective-permute-start = (bf16[8,512]{1,0:T(8,128)(2,1)S(1)}, bf16[8,512]{1,0:T(8,128)(2,1)S(1)}, u32[]{:S(2)}, u32[]{:S(2)}) collective-permute-start(bf16[8,512]{1,0:T(8,128)(2,1)S(1)} %get-tuple-element.10), channel_id=1, source_target_pairs={{0,1},{1,2},{2,3},{3,4},{4,5},{5,6},{6,7},{7,8},{8,9},{9,10},{10,1... | collective-permute-start | bytes 24584 | tf_op jit(solution)/shard_map/ppermute | solution.py:20
  54.0 1.9 %collective-permute-start.1 = (bf16[8,512]{1,0:T(8,128)(2,1)S(1)}, bf16[8,512]{1,0:T(8,128)(2,1)S(1)}, u32[]{:S(2)}, u32[]{:S(2)}) collective-permute-start(bf16[8,512]{1,0:T(8,128)(2,1)S(1)} %get-tuple-element.11), channel_id=1, source_target_pairs={{1,0},{2,1},{3,2},{4,3},{5,4},{6,5},{7,6},{8,7},{9,8},{10,9},{11,1... | collective-permute-start | bytes 24584 | tf_op jit(solution)/shard_map/ppermute | solution.py:23
  56.2 0.5 broadcast_compare_fusion.5
  56.7 0.6 broadcast_compare_fusion.7
  57.3 0.6 broadcast_compare_fusion.9
  57.9 0.6 broadcast_compare_fusion.11
  58.5 0.6 broadcast_compare_fusion.13
  59.1 0.6 broadcast_compare_fusion.15
  59.7 0.6 broadcast_compare_fusion.17
  60.2 0.6 broadcast_compare_fusion.19
  60.8 0.6 broadcast_compare_fusion.21
  61.4 0.6 broadcast_compare_fusion.23
  62.0 0.6 broadcast_compare_fusion.25
  62.6 0.6 broadcast_compare_fusion.27
  63.2 0.1 copy.17
  63.4 0.1 copy.18
  63.6 0.1 eq.238
  63.6 0.0 copy-done.7
  63.6 1.1 multiply_bitcast_fusion
  64.8 5.6 %fusion.4 = f32[512,896]{1,0:T(8,128)} fusion(bf16[512,2048]{1,0:T(8,128)(2,1)S(1)} %bitcast.42, bf16[1,2048,896]{2,1,0:T(8,128)(2,1)} %param.23), kind=kOutput, calls=%fused_computation.4 | convolution fusion | flops 1879048192 | bytes 7602176 | tf_op jit(solution)/shard_map/dot_general | solution.py:444
  70.4 9.5 %fusion.6 = bf16[512,2048]{1,0:T(8,128)(2,1)} fusion(bf16[1,896,2048]{2,1,0:T(8,128)(2,1)} %param.25, f32[512,896]{1,0:T(8,128)} %fusion.4, bf16[512,2048]{1,0:T(8,128)(2,1)S(1)} %bitcast.43, bf16[1,2048,896]{2,1,0:T(8,128)(2,1)} %param.24), kind=kOutput, calls=%fused_computation.6 | convolution fusion | flops 3761897472 | bytes 13369344 | tf_op jit(solution)/shard_map/dot_general | solution.py:447
  80.0 1.6 %copy-done.2 = bf16[512,2048]{1,0:T(8,128)(2,1)S(1)} copy-done((bf16[512,2048]{1,0:T(8,128)(2,1)S(1)}, bf16[512,2048]{1,0:T(8,128)(2,1)}, u32[]{:S(2)}) %copy-start.2) | copy-done | bytes 2097176
  81.6 30.7 %combine.1 = bf16[128,2048]{1,0:T(8,128)(2,1)S(1)} custom-call(bf16[8,64,2048]{2,1,0:T(8,128)(2,1)S(1)} %bitcast.44, f32[128,512]{1,0:T(8,128)S(1)} %compare_select_fusion.refs_1_), custom_call_target="tpu_custom_call" | custom-call | flops 1000000000 | bytes 2097152 | tf_op jit(solution)/shard_map/combine/pallas_call | solution.py:393
  112.3 1.9 %reshape.527 = bf16[512,512]{1,0:T(8,128)(2,1)S(1)} reshape(bf16[8,64,8,64]{3,2,1,0:T(8,128)(2,1)} %multiply_bitcast_fusion) | data formatting | bytes 1048576 | tf_op jit(solution)/shard_map/reshape | solution.py:66
  114.2 0.0 collective-permute-done
  114.2 0.0 collective-permute-done.1
  114.3 0.9 maximum_convert_fusion
  115.2 3.4 %convolution_convert_fusion = bf16[128,2048]{1,0:T(8,128)(2,1)} fusion(bf16[512,2048]{1,0:T(8,128)(2,1)S(1)} %copy-done.4, bf16[512,512]{1,0:T(8,128)(2,1)S(1)} %reshape.527, f32[144,512]{1,0:T(8,128)S(1)} %maximum_convert_fusion, f32[512]{0:T(512)S(1)} %copy-done.10, f32[512]{0:T(512)S(1)} %get-tuple-element.61, pred[512]{0:T(512)(128)(4,1)S(1)} %get-tuple-element.31, ...), kind=kOutput, calls=%fused_computation.7 | convolution fusion | flops 342097920 | bytes 7367680 | tf_op jit(solution)/shard_map/dot_general | solution.py:70
  118.7 0.8 copy.22
  (35 shorter events, 0.3 us)
Async XLA Ops:
  0.6 5.1 %copy-start = (bf16[2048,128]{1,0:T(8,128)(2,1)S(1)}, bf16[2048,128]{1,0:T(8,128)(2,1)}, u32[]{:S(2)}) copy-start(bf16[2048,128]{1,0:T(8,128)(2,1)} %refs_1_.1) | copy-start | bytes 1572868
  0.6 5.1 %copy-start.1 = (bf16[128,2048]{1,0:T(8,128)(2,1)S(1)}, bf16[128,2048]{1,0:T(8,128)(2,1)}, u32[]{:S(2)}) copy-start(bf16[128,2048]{1,0:T(8,128)(2,1)} %refs_2_.1) | copy-start | bytes 1572868
  5.7 43.1 %copy-start.5 = (bf16[128,2048]{1,0:T(8,128)(2,1)S(1)}, bf16[128,2048]{1,0:T(8,128)(2,1)}, u32[]{:S(2)}) copy-start(bf16[128,2048]{1,0:T(8,128)(2,1)} %param.13) | copy-start | bytes 1572868
  5.7 43.1 %copy-start.9 = (f32[2048]{0:T(1024)S(1)}, f32[2048]{0:T(1024)}, u32[]{:S(2)}) copy-start(f32[2048]{0:T(1024)} %param.14) | copy-start | bytes 24580
  48.8 1.3 %copy-start.3 = (bf16[512,2048]{1,0:T(8,128)(2,1)}, bf16[512,2048]{1,0:T(8,128)(2,1)S(1)}, u32[]{:S(2)}) copy-start(bf16[512,2048]{1,0:T(8,128)(2,1)S(1)} %get-tuple-element.6) | copy-start | bytes 6291460
  48.8 14.6 %copy-start.8 = (f32[128,2]{0,1:T(2,128)S(1)}, f32[128,2]{0,1:T(2,128)}, u32[]{:S(2)}) copy-start(f32[128,2]{0,1:T(2,128)} %param.22) | copy-start | bytes 3076
  48.8 14.8 %copy-start.7 = (bf16[8,64,64]{2,1,0:T(8,128)(2,1)S(1)}, bf16[8,64,64]{2,1,0:T(8,128)(2,1)}, u32[]{:S(2)}) copy-start(bf16[8,64,64]{2,1,0:T(8,128)(2,1)} %param.16) | copy-start | bytes 196612
  50.1 0.7 copy-start.6
  50.8 63.5 %collective-permute-start = (bf16[8,512]{1,0:T(8,128)(2,1)S(1)}, bf16[8,512]{1,0:T(8,128)(2,1)S(1)}, u32[]{:S(2)}, u32[]{:S(2)}) collective-permute-start(bf16[8,512]{1,0:T(8,128)(2,1)S(1)} %get-tuple-element.10), channel_id=1, source_target_pairs={{0,1},{1,2},{2,3},{3,4},{4,5},{5,6},{6,7},{7,8},{8,9},{9,10},{10,1... | collective-permute-start | bytes 24584 | tf_op jit(solution)/shard_map/ppermute | solution.py:20
  54.0 60.3 %collective-permute-start.1 = (bf16[8,512]{1,0:T(8,128)(2,1)S(1)}, bf16[8,512]{1,0:T(8,128)(2,1)S(1)}, u32[]{:S(2)}, u32[]{:S(2)}) collective-permute-start(bf16[8,512]{1,0:T(8,128)(2,1)S(1)} %get-tuple-element.11), channel_id=1, source_target_pairs={{1,0},{2,1},{3,2},{4,3},{5,4},{6,5},{7,6},{8,7},{9,8},{10,9},{11,1... | collective-permute-start | bytes 24584 | tf_op jit(solution)/shard_map/ppermute | solution.py:23
  80.0 1.6 %copy-start.2 = (bf16[512,2048]{1,0:T(8,128)(2,1)S(1)}, bf16[512,2048]{1,0:T(8,128)(2,1)}, u32[]{:S(2)}) copy-start(bf16[512,2048]{1,0:T(8,128)(2,1)} %fusion.6) | copy-start | bytes 6291460
  81.6 33.6 %copy-start.4 = (bf16[512,2048]{1,0:T(8,128)(2,1)S(1)}, bf16[512,2048]{1,0:T(8,128)(2,1)}, u32[]{:S(2)}) copy-start(bf16[512,2048]{1,0:T(8,128)(2,1)} %copy-done.3) | copy-start | bytes 6291460
  81.6 33.6 %copy-start.10 = (f32[512]{0:T(512)S(1)}, f32[512]{0:T(512)}, u32[]{:S(2)}) copy-start(f32[512]{0:T(512)} %param.17) | copy-start | bytes 6148
